TPU v7x, 32 devices: a whole 2x2x4 slice. The times are simulated.
32 devices in a mesh: ep: 8 (over z, y), tp: 4 (over x, core).
Axes of the slice: x: 2, y: 2, z: 4, core: 2. Of those that a mesh axis runs over, the one named last changes fastest.
Arguments:
- tokens: bfloat16 [192, 1024], P('ep'), may hold values from -3 to 3
- attn_gain: float32 [1024], replicated, may hold values from 0.1 to 1.9
- w_query: bfloat16 [1024, 1024], P(None, 'tp'), may hold values from -0.1875 to 0.1875
- w_key: bfloat16 [1024, 256], P(None, 'tp'), may hold values from -0.1875 to 0.1875
- w_value: bfloat16 [1024, 256], P(None, 'tp'), may hold values from -0.1875 to 0.1875
- attn_bias: float32 [16], P('tp'), may hold values from -7.5 to -3
- key_cache: bfloat16 [192, 256, 1024], P('ep', 'tp'), may hold values from -6 to 6
- value_cache: bfloat16 [192, 256, 1024], P('ep', 'tp'), may hold values from -6 to 6
- lengths: int32 [192], P('ep'), may hold values from 128 to 1024
- w_out: bfloat16 [1024, 1024], P('tp'), may hold values from -0.75 to 0.75
- ffn_gain: float32 [1024], replicated, may hold values from 0.1 to 1.9
- routes: int32 [192, 2], P('ep'), may hold values from 0 to 7, all different within a row; in each aligned block of 24 rows (0 to 23, 24 to 47, ...) at most 12 rows name the same one
- route_weight: float32 [192, 2], P('ep'), may hold values from 0.2 to 1
- expert_gate: bfloat16 [8, 1024, 3584], P('ep', None, 'tp'), may hold values from -0.1875 to 0.1875
- expert_up: bfloat16 [8, 1024, 3584], P('ep', None, 'tp'), may hold values from -0.1875 to 0.1875
- expert_down: bfloat16 [8, 3584, 1024], P('ep', 'tp'), may hold values from -0.09375 to 0.09375
Outputs:
- mixed: bfloat16 [192, 1024], P('ep')
- new_keys: bfloat16 [192, 256], P('ep', 'tp')
- new_values: bfloat16 [192, 256], P('ep', 'tp')
Inputs may be any that keep to these rules, and one draw needn't show every extreme that they name: `routes`: each row names 2 different experts. Among the rows of one device no expert is named by more than 12 of them, and on some device some expert is named by exactly 12.
All inputs are finite; a program needn't handle non-finite values.
Results may differ from a plain program's by a relative error of at most 0.02.
Values may be sent and summed in bfloat16 or wider, within the bound.
A program may use at most 64 MiB of HBM per device.

v0:
```python
import functools

import jax
import jax.numpy as jnp
from jax import lax
from jax.experimental import pallas as pl
from jax.experimental.pallas import tpu as pltpu
from jax.sharding import PartitionSpec as P

EPS = 1e-06
F32 = jnp.float32
BF16 = jnp.bfloat16
MESH = pl.DeviceIdType.MESH
CUT = False


def iota(shape, dim):
    return lax.broadcasted_iota(jnp.int32, shape, dim)


def onehot(mask):
    return jnp.where(mask, 1.0, 0.0).astype(BF16)


def dot(a, b):
    return jnp.dot(a, b, preferred_element_type=F32)


def dot_nt(a, b):
    return lax.dot_general(a, b, (((1,), (1,)), ((), ())), preferred_element_type=F32)


def rms(x, gains):
    factor = lax.rsqrt(jnp.mean(x * x, axis=-1, keepdims=True) + EPS)
    return (x * factor * gains).astype(BF16)


def kernel(
    n_ep, n_tp, capacity, cap_pad,
    tokens, attn_gain, w_query, w_key, w_value, attn_bias, key_cache, value_cache, lengths,
    w_out, ffn_gain, routes, route_weight, gate, up, down,
    mixed, new_keys, new_values,
    wq, wk, wv, kbuf, vbuf, wo, wg, wu, wd,
    part, parts, outgoing, arrived, passed, shares, share_in, ret, back, own_share, gathered,
    load_sem, k_sem, v_sem,
    a_send, a_recv, b_send, b_recv, f_send, f_recv, c_send, c_recv, d_send, d_recv, e_send, e_recv,
):
    ep = lax.axis_index("ep")
    tp = lax.axis_index("tp")
    seqs, width = tokens.shape
    head = w_key.shape[0]
    heads = w_query.shape[1] // head
    span = key_cache.shape[2]
    rows = seqs * heads
    per_group = max(1, 256 // head)
    while seqs % per_group:
        per_group //= 2
    groups = seqs // per_group
    quarter = width // n_tp
    total = n_ep * cap_pad

    loads = {}
    for i, (name, src, dst) in enumerate(
        (("wq", w_query, wq), ("wk", w_key, wk), ("wv", w_value, wv), ("wo", w_out, wo),
         ("wg", gate.at[0], wg), ("wu", up.at[0], wu), ("wd", down.at[0], wd))
    ):
        loads[name] = pltpu.make_async_copy(src, dst, load_sem.at[i])
    k_loads, v_loads = [], []
    for g in range(groups):
        piece = pl.ds(g * per_group, per_group)
        k_loads.append(pltpu.make_async_copy(key_cache.at[piece], kbuf.at[piece], k_sem.at[g]))
        v_loads.append(pltpu.make_async_copy(value_cache.at[piece], vbuf.at[piece], v_sem.at[g]))
    loads["wq"].start()
    for c in k_loads:
        c.start()
    for c in v_loads:
        c.start()
    for name in ("wo", "wg", "wu", "wd", "wk", "wv"):
        loads[name].start()

    barrier = pltpu.get_barrier_semaphore()
    for d in range(1, n_tp):
        pl.semaphore_signal(barrier, inc=1, device_id=(ep, lax.rem(tp + d, n_tp)), device_id_type=MESH)
    for d in range(1, n_ep):
        pl.semaphore_signal(barrier, inc=1, device_id=(lax.rem(ep + d, n_ep), tp), device_id_type=MESH)

    token_rows = tokens[...].astype(F32)
    normed = rms(token_rows, attn_gain[...])

    loads["wq"].wait()
    queries = dot(normed, wq[...]).astype(BF16)
    q_cols = heads * head
    g_cols = per_group * head
    repeat = onehot(iota((rows, seqs), 0) // heads == iota((rows, seqs), 1))
    spread = dot(repeat, queries)
    head_mask = iota((rows, q_cols), 0) % heads == iota((rows, q_cols), 1) // head
    seq_mask = (iota((rows, g_cols), 0) // heads) % per_group == iota((rows, g_cols), 1) // head
    fold_q = onehot(iota((q_cols, g_cols), 0) % head == iota((q_cols, g_cols), 1) % head)
    spread = jnp.where(head_mask, spread, 0.0).astype(BF16)
    diag = jnp.where(seq_mask, dot(spread, fold_q), 0.0).astype(BF16)

    g_rows = per_group * heads
    pieces = []
    for g in range(groups):
        k_loads[g].wait()
        block = kbuf[g * per_group:(g + 1) * per_group].reshape(g_cols, span)
        pieces.append(dot(diag[g * g_rows:(g + 1) * g_rows], block))
    scores = jnp.concatenate(pieces, axis=0) * (head ** -0.5)

    pick = iota((rows, heads), 0) % heads == iota((rows, heads), 1)
    bias_col = jnp.sum(jnp.where(pick, attn_bias[...], 0.0), axis=1, keepdims=True)
    pick = iota((rows, seqs), 0) // heads == iota((rows, seqs), 1)
    len_col = jnp.sum(jnp.where(pick, lengths[...].astype(F32), 0.0), axis=1, keepdims=True)
    scores = scores + bias_col
    inside = iota((rows, span), 1).astype(F32) < len_col
    soft = jnp.log(1.0 + jnp.exp(-jnp.abs(scores)))
    fall = jnp.where(inside, -(jnp.maximum(scores, 0.0) + soft), 0.0)
    rise = jnp.minimum(scores, 0.0) - soft
    high = fall.astype(BF16)
    low = (fall - high.astype(F32)).astype(BF16)
    block_len = 256 if span % 256 == 0 else span
    blocks = span // block_len
    later = onehot(iota((block_len, block_len), 0) > iota((block_len, block_len), 1))
    stacked = jnp.concatenate(
        [x[:, j * block_len:(j + 1) * block_len] for j in range(blocks) for x in (high, low)], axis=0)
    suffix = dot(stacked, later)
    weights = [None] * blocks
    offset = jnp.zeros((rows, 1), F32)
    for j in reversed(range(blocks)):
        cols = slice(j * block_len, (j + 1) * block_len)
        after = suffix[2 * j * rows:(2 * j + 1) * rows] + suffix[(2 * j + 1) * rows:(2 * j + 2) * rows]
        w = jnp.exp(rise[:, cols] + (after + offset))
        weights[j] = jnp.where(inside[:, cols], w, 0.0).astype(BF16)
        offset = offset + after[:, 0:1] + fall[:, j * block_len:j * block_len + 1]
    weights = jnp.concatenate(weights, axis=1)

    pieces = []
    for g in range(groups):
        v_loads[g].wait()
        block = vbuf[g * per_group:(g + 1) * per_group].reshape(g_cols, span)
        pieces.append(dot_nt(weights[g * g_rows:(g + 1) * g_rows], block))
    attended = jnp.where(seq_mask, jnp.concatenate(pieces, axis=0), 0.0).astype(BF16)
    fold_o = onehot(iota((g_cols, q_cols), 0) % head == iota((g_cols, q_cols), 1) % head)
    attended = jnp.where(head_mask, dot(attended, fold_o), 0.0).astype(BF16)
    gather = onehot(iota((seqs, rows), 0) == iota((seqs, rows), 1) // heads)
    attended = dot(gather, attended).astype(BF16)

    loads["wo"].wait()
    part[...] = dot(attended, wo[...]).astype(BF16)

    pl.semaphore_wait(barrier, n_tp - 1 + n_ep - 1)
    sends = []
    for d in range(1, n_tp):
        peer = lax.rem(tp + d, n_tp)
        c = pltpu.make_async_remote_copy(
            part, parts.at[tp], a_send.at[d], a_recv.at[tp], device_id=(ep, peer), device_id_type=MESH)
        c.start()
        sends.append(c)

    first = routes[0:1, :] == iota((total, seqs), 0) // cap_pad
    named = first | (routes[1:2, :] == iota((total, seqs), 0) // cap_pad)
    earlier = onehot(iota((seqs, seqs), 0) < iota((seqs, seqs), 1))
    before = dot(onehot(named), earlier)
    slot_of = iota((total, seqs), 0) % cap_pad
    planned = jnp.where(named & (before == slot_of.astype(F32)), 1.0, 0.0)
    plan = planned.astype(BF16)
    mixing = (planned * jnp.where(first, route_weight[0:1, :], route_weight[1:2, :])).T
    mix_high = mixing.astype(BF16)
    mix_low = (mixing - mix_high.astype(F32)).astype(BF16)
    loads["wk"].wait()
    loads["wv"].wait()
    new_keys[...] = dot_nt(normed, wk[...]).astype(BF16)
    new_values[...] = dot_nt(normed, wv[...]).astype(BF16)

    attn_total = part[...].astype(F32)
    for d in range(1, n_tp):
        src = lax.rem(tp + n_tp - d, n_tp)
        pltpu.make_async_remote_copy(
            part, parts.at[src], a_send.at[d], a_recv.at[src], device_id=(ep, src), device_id_type=MESH
        ).wait_recv()
        attn_total = attn_total + parts[src].astype(F32)
    residual = (token_rows + attn_total).astype(BF16)
    normed_two = rms(residual.astype(F32), ffn_gain[...])
    half = width // 2
    core = lax.rem(tp, 2)
    mate = tp + 1 - 2 * core
    mine = jnp.where(core == 0, normed_two[:, :half], normed_two[:, half:])
    outgoing[...] = dot(plan, mine).astype(BF16).reshape(n_ep, cap_pad, half)

    def cut(ref, *index):
        return ref.at[index + (pl.ds(0, capacity),)] if CUT else ref.at[index]

    for d in range(1, n_ep):
        peer = lax.rem(ep + d, n_ep)
        c = pltpu.make_async_remote_copy(
            cut(outgoing, peer), cut(arrived, ep), b_send.at[d], b_recv.at[ep],
            device_id=(peer, tp), device_id_type=MESH)
        c.start()
        sends.append(c)
    c = pltpu.make_async_remote_copy(
        cut(outgoing, ep), cut(passed, ep), f_send.at[0], f_recv.at[ep], device_id=(ep, mate), device_id_type=MESH)
    c.start()
    sends.append(c)
    swaps = [c]
    arrived[ep] = outgoing[ep]
    loads["wg"].wait()
    loads["wu"].wait()
    for d in range(1, n_ep):
        src = lax.rem(ep + n_ep - d, n_ep)
        pltpu.make_async_remote_copy(
            cut(outgoing, src), cut(arrived, src), b_send.at[d], b_recv.at[src],
            device_id=(src, tp), device_id_type=MESH).wait_recv()
        c = pltpu.make_async_remote_copy(
            cut(arrived, src), cut(passed, src), f_send.at[d], f_recv.at[src],
            device_id=(ep, mate), device_id_type=MESH)
        c.start()
        sends.append(c)
        swaps.append(c)
    kept = iota((total, 1), 0) % cap_pad < capacity

    def clean(x):
        return jnp.where(kept, x, jnp.zeros_like(x)) if CUT else x

    at_own = pl.ds(pl.multiple_of(core * half, half), half)
    at_mate = pl.ds(pl.multiple_of((1 - core) * half, half), half)
    x = clean(arrived[...].reshape(total, half))
    gated = dot(x, wg[at_own, :])
    lifted = dot(x, wu[at_own, :])
    for c in swaps:
        c.wait_recv()
    x = clean(passed[...].reshape(total, half))
    gated = gated + dot(x, wg[at_mate, :])
    lifted = lifted + dot(x, wu[at_mate, :])
    loads["wd"].wait()
    hidden = (gated / (1.0 + jnp.exp(-gated)) * lifted).astype(BF16)
    for d in list(range(1, n_tp)) + [0]:
        peer = lax.rem(tp + d, n_tp)
        at = pl.ds(pl.multiple_of(peer * quarter, quarter), quarter)
        value = dot(hidden, wd[:, at]).astype(BF16)
        if d == 0:
            summed = value.astype(F32)
            break
        shares[d] = value.reshape(n_ep, cap_pad, quarter)
        c = pltpu.make_async_remote_copy(
            shares.at[d, :, pl.ds(0, capacity)] if CUT else shares.at[d],
            share_in.at[tp, :, pl.ds(0, capacity)] if CUT else share_in.at[tp], c_send.at[d], c_recv.at[tp],
            device_id=(ep, peer), device_id_type=MESH)
        c.start()
        sends.append(c)
    for d in range(1, n_tp):
        src = lax.rem(tp + n_tp - d, n_tp)
        pltpu.make_async_remote_copy(
            shares.at[d, :, pl.ds(0, capacity)] if CUT else shares.at[d],
            share_in.at[src, :, pl.ds(0, capacity)] if CUT else share_in.at[src], c_send.at[d], c_recv.at[src],
            device_id=(ep, src), device_id_type=MESH).wait_recv()
        summed = summed + clean(share_in[src].reshape(total, quarter)).astype(F32)
    ret[...] = summed.astype(BF16).reshape(n_ep, cap_pad, quarter)

    for d in range(1, n_ep):
        peer = lax.rem(ep + d, n_ep)
        c = pltpu.make_async_remote_copy(
            cut(ret, peer), cut(back, ep), d_send.at[d], d_recv.at[ep],
            device_id=(peer, tp), device_id_type=MESH)
        c.start()
        sends.append(c)
    back[ep] = ret[ep]
    own = jnp.zeros((seqs, quarter), F32)
    for t in range(n_tp):
        own = jnp.where(tp == t, residual[:, t * quarter:(t + 1) * quarter].astype(F32), own)
    for d in range(1, n_ep):
        src = lax.rem(ep + n_ep - d, n_ep)
        pltpu.make_async_remote_copy(
            cut(ret, src), cut(back, src), d_send.at[d], d_recv.at[src],
            device_id=(src, tp), device_id_type=MESH).wait_recv()
    flat = clean(back[...].reshape(total, quarter))
    share = (own + (dot(mix_high, flat) + dot(mix_low, flat))).astype(BF16)
    own_share[...] = share
    gathered[tp] = share
    for d in range(1, n_tp):
        peer = lax.rem(tp + d, n_tp)
        c = pltpu.make_async_remote_copy(
            own_share, gathered.at[tp], e_send.at[d], e_recv.at[tp],
            device_id=(ep, peer), device_id_type=MESH)
        c.start()
        sends.append(c)
    for d in range(1, n_tp):
        src = lax.rem(tp + n_tp - d, n_tp)
        pltpu.make_async_remote_copy(
            own_share, gathered.at[src], e_send.at[d], e_recv.at[src],
            device_id=(ep, src), device_id_type=MESH).wait_recv()
    for t in range(n_tp):
        mixed[:, t * quarter:(t + 1) * quarter] = gathered[t]
    for c in sends:
        c.wait_send()


def finish(mixed_in, keys_in, values_in, mixed, keys, values):
    mixed[...] = mixed_in[...]
    keys[...] = keys_in[...]
    values[...] = values_in[...]


def solution(mesh):
    n_ep, n_tp = mesh.shape["ep"], mesh.shape["tp"]

    def body(tokens, attn_gain, w_query, w_key, w_value, attn_bias, key_cache, value_cache, lengths,
             w_out, ffn_gain, routes, route_weight, gate, up, down):
        seqs, width = tokens.shape
        top = routes.shape[1]
        capacity = max(2, 2 * seqs * top // n_ep)
        cap_pad = -(-capacity // 16) * 16
        quarter = width // n_tp
        head = w_key.shape[1]
        units = gate.shape[2]
        groups = seqs
        vmem = pl.BlockSpec(memory_space=pltpu.VMEM)
        hbm = pl.BlockSpec(memory_space=pl.ANY)
        sem = pltpu.SemaphoreType.DMA
        outs = pl.pallas_call(
            functools.partial(kernel, n_ep, n_tp, capacity, cap_pad),
            out_shape=(
                jax.ShapeDtypeStruct((seqs, width), BF16),
                jax.ShapeDtypeStruct((seqs, head), BF16),
                jax.ShapeDtypeStruct((seqs, head), BF16),
            ),
            in_specs=[vmem, vmem, hbm, hbm, hbm, vmem, hbm, hbm, vmem, hbm, vmem, vmem, vmem, hbm, hbm, hbm],
            out_specs=(vmem, vmem, vmem),
            scratch_shapes=[
                pltpu.VMEM(w_query.shape, BF16),
                pltpu.VMEM((head, width), BF16),
                pltpu.VMEM((head, width), BF16),
                pltpu.VMEM(key_cache.shape, BF16),
                pltpu.VMEM(value_cache.shape, BF16),
                pltpu.VMEM(w_out.shape, BF16),
                pltpu.VMEM((width, units), BF16),
                pltpu.VMEM((width, units), BF16),
                pltpu.VMEM((units, width), BF16),
                pltpu.VMEM((seqs, width), BF16),
                pltpu.VMEM((n_tp, seqs, width), BF16),
                pltpu.VMEM((n_ep, cap_pad, width // 2), BF16),
                pltpu.VMEM((n_ep, cap_pad, width // 2), BF16),
                pltpu.VMEM((n_ep, cap_pad, width // 2), BF16),
                pltpu.VMEM((n_tp, n_ep, cap_pad, quarter), BF16),
                pltpu.VMEM((n_tp, n_ep, cap_pad, quarter), BF16),
                pltpu.VMEM((n_ep, cap_pad, quarter), BF16),
                pltpu.VMEM((n_ep, cap_pad, quarter), BF16),
                pltpu.VMEM((seqs, quarter), BF16),
                pltpu.VMEM((n_tp, seqs, quarter), BF16),
                sem((7,)), sem((groups,)), sem((groups,)),
                sem((n_tp,)), sem((n_tp,)), sem((n_ep,)), sem((n_ep,)), sem((n_ep,)), sem((n_ep,)),
                sem((n_tp,)), sem((n_tp,)), sem((n_ep,)), sem((n_ep,)), sem((n_tp,)), sem((n_tp,)),
            ],
            compiler_params=pltpu.CompilerParams(
                collective_id=0, has_side_effects=True, vmem_limit_bytes=60 * 1024 * 1024),
        )(tokens, attn_gain[None, :], w_query, w_key.T, w_value.T, attn_bias[None, :], key_cache, value_cache,
          lengths[None, :], w_out, ffn_gain[None, :], routes.T, route_weight.T, gate, up, down)
        return pl.pallas_call(
            finish,
            out_shape=tuple(jax.ShapeDtypeStruct(x.shape, x.dtype) for x in outs),
            in_specs=[vmem] * 3,
            out_specs=(vmem,) * 3,
        )(*outs)

    return jax.shard_map(
        body,
        mesh=mesh,
        in_specs=(
            P("ep", None), P(), P(None, "tp"), P(None, "tp"), P(None, "tp"), P("tp"),
            P("ep", "tp", None), P("ep", "tp", None), P("ep"), P("tp", None), P(),
            P("ep", None), P("ep", None),
            P("ep", None, "tp"), P("ep", None, "tp"), P("ep", "tp", None),
        ),
        out_specs=(P("ep", None), P("ep", "tp"), P("ep", "tp")),
        check_vma=False,
    )
```

profile of v0, /device:TPU:0, one launch (start us, length us, event | category | flops | bytes accessed | tf_op | source)
XLA Modules:
  0.0 37.6 jit_solution(15819962411039303026)
XLA Ops:
  0.6 35.5 %shard_map.175 = (bf16[24,1024]{1,0:T(8,128)(2,1)}, bf16[24,64]{1,0:T(8,128)(2,1)}, bf16[24,64]{1,0:T(8,128)(2,1)}) custom-call(bf16[24,1024]{1,0:T(8,128)(2,1)} %tokens.1, f32[1,1024]{1,0:T(1,128)} %bitcast.10, bf16[1024,256]{1,0:T(8,128)(2,1)} %w_query.1, bf16[64,1024]{1,0:T(8,128)(2,1)} %bitcast.8, bf16[64,1024]{1,0:T(8,128)(2,1)} %bitcast.9, ...), custom_call_target="tpu_custom_call" | custom-call | tf_op jit(solution)/shard_map/pallas_call | solution.py:319
  36.1 1.4 %shard_map.176 = (bf16[24,1024]{1,0:T(8,128)(2,1)}, bf16[24,64]{1,0:T(8,128)(2,1)}, bf16[24,64]{1,0:T(8,128)(2,1)}) custom-call(bf16[24,1024]{1,0:T(8,128)(2,1)} %get-tuple-element.6.mixed_in, bf16[24,64]{1,0:T(8,128)(2,1)} %get-tuple-element.7.keys_in, bf16[24,64]{1,0:T(8,128)(2,1)} %get-tuple-element.8.values_in), custom_call_target="tpu_custom_call" | custom-call | tf_op jit(solution)/shard_map/pallas_call | solution.py:357
where the time goes:
time: 37.8 us; the launch traced here: 37.6 us
  Pallas kernels  37 us (98%)
  between operations  0.65 us (2%)
    pallas_call x1, Pallas kernels, body(): pl.pallas_call(functools.partial(kernel, n_ep, n_tp, capacity, cap_pad),...  35.5 us
    pallas_call x1, Pallas kernels, body(): pl.pallas_call(finish, out_shape=tuple((jax.ShapeDtypeStruct(x.shape, x.d...  1.45 us

commit v1 on v0

v1 whole, which is shorter than its diff:
```python
import functools

import jax
import jax.numpy as jnp
from jax import lax
from jax.experimental import pallas as pl
from jax.experimental.pallas import tpu as pltpu
from jax.sharding import PartitionSpec as P

EPS = 1e-06
F32 = jnp.float32
BF16 = jnp.bfloat16
MESH = pl.DeviceIdType.MESH


def iota(shape, dim):
    return lax.broadcasted_iota(jnp.int32, shape, dim)


def onehot(mask):
    return jnp.where(mask, 1.0, 0.0).astype(BF16)


def dot(a, b):
    return jnp.dot(a, b, preferred_element_type=F32)


def dot_nt(a, b):
    return lax.dot_general(a, b, (((1,), (1,)), ((), ())), preferred_element_type=F32)


def kernel(
    n_ep, n_tp, capacity, cap_pad,
    tokens_hbm, attn_gain_hbm, w_query, w_key, w_value, attn_bias_hbm, key_cache, value_cache, lengths_hbm,
    w_out, ffn_gain_hbm, routes_hbm, route_weight_hbm, gate, up, down,
    mixed, new_keys, new_values,
    tokens, attn_gain, attn_bias, lengths, ffn_gain, routes, route_weight,
    wq, wk, wv, kbuf, vbuf, wo, wg, wu, wd,
    part, parts, outgoing, arrived, passed, share_out, share_in, ret, back, fin_out, finals,
    load_sem, k_sem, v_sem,
    a_send, a_recv, b_send, b_recv, f_send, f_recv, c_send, c_recv, d_send, d_recv, e_send, e_recv,
):
    ep = lax.axis_index("ep")
    tp = lax.axis_index("tp")
    seqs, width = tokens.shape
    head = w_key.shape[0]
    heads = w_query.shape[1] // head
    span = key_cache.shape[2]
    rows = seqs * heads
    depth = seqs * head
    half = width // 2
    total = n_ep * cap_pad
    core = lax.rem(tp, 2)
    mate = tp + 1 - 2 * core
    lanes = 128
    per = lanes // head
    chunks = depth // lanes

    pow2 = n_ep & (n_ep - 1) == 0

    def dest(k):
        if not pow2:
            return lax.rem(ep + k, n_ep)
        other, bit = ep, 1
        while bit < n_ep:
            if k & bit:
                other = other + bit * (1 - 2 * lax.rem(ep // bit, 2))
            bit *= 2
        return other

    def source(k):
        return dest(k) if pow2 else lax.rem(ep + n_ep - k, n_ep)

    loads = {}
    for i, (name, src, dst) in enumerate(
        (("tokens", tokens_hbm, tokens), ("gain", attn_gain_hbm, attn_gain), ("wq", w_query, wq),
         ("bias", attn_bias_hbm, attn_bias), ("lengths", lengths_hbm, lengths), ("fgain", ffn_gain_hbm, ffn_gain),
         ("routes", routes_hbm, routes), ("weights", route_weight_hbm, route_weight),
         ("wk", w_key, wk), ("wv", w_value, wv), ("wo", w_out, wo),
         ("wg", gate.at[0], wg), ("wu", up.at[0], wu), ("wd", down.at[0], wd))
    ):
        loads[name] = pltpu.make_async_copy(src, dst, load_sem.at[i])
    k_parts, v_parts = k_sem.shape[0], k_sem.shape[1]
    k_cols = span // k_parts
    k_rows = seqs // v_parts
    k_loads, v_loads = [], []
    for a in range(k_parts):
        at = pl.ds((k_parts - 1 - a) * k_cols, k_cols)
        k_loads.append([])
        for b in range(v_parts):
            piece = pl.ds(b * k_rows, k_rows)
            k_loads[-1].append(
                pltpu.make_async_copy(key_cache.at[piece, :, at], kbuf.at[piece, :, at], k_sem.at[a, b]))
    for b in range(v_sem.shape[0]):
        piece = pl.ds(b * (seqs // v_sem.shape[0]), seqs // v_sem.shape[0])
        v_loads.append(pltpu.make_async_copy(value_cache.at[piece], vbuf.at[piece], v_sem.at[b]))
    for name in ("tokens", "gain", "wq"):
        loads[name].start()
    for c in k_loads[0]:
        c.start()
    for name in ("bias", "lengths"):
        loads[name].start()
    for group in k_loads[1:]:
        for c in group:
            c.start()

    barrier = pltpu.get_barrier_semaphore()
    for d in range(1, n_tp):
        pl.semaphore_signal(barrier, inc=1, device_id=(ep, lax.rem(tp + d, n_tp)), device_id_type=MESH)
    for k in range(1, n_ep):
        pl.semaphore_signal(barrier, inc=1, device_id=(dest(k), tp), device_id_type=MESH)

    loads["tokens"].wait()
    loads["gain"].wait()
    token_rows = tokens[...].astype(F32)
    factor = lax.rsqrt(jnp.mean(token_rows * token_rows, axis=-1, keepdims=True) + EPS)
    normed = (token_rows * factor * attn_gain[...]).astype(BF16)

    loads["wq"].wait()
    for c in v_loads:
        c.start()
    queries = dot(normed, wq[...]) * (head ** -0.5)
    block_of = iota((seqs, lanes), 1) // head
    seq_of = iota((seqs, lanes), 0)
    spread = []
    for h in range(heads):
        pair = queries[:, (h // per) * lanes:(h // per + 1) * lanes]
        mine = jnp.zeros_like(pair)
        for j in range(per):
            shift = ((j - h % per) * head) % lanes
            turned = pltpu.roll(pair, shift, 1) if shift else pair
            mine = jnp.where(block_of == j, turned, mine)
        spread.append(mine)
    masks = [seq_of == block_of + c * per for c in range(chunks)]
    diag = jnp.concatenate(
        [jnp.concatenate([jnp.where(m, q, 0.0) for m in masks], axis=1) for q in spread], axis=0).astype(BF16)

    loads["bias"].wait()
    loads["lengths"].wait()
    bias_col = jnp.concatenate(
        [jnp.broadcast_to(attn_bias[0:1, h:h + 1], (seqs, 1)) for h in range(heads)], axis=0)
    same = iota((seqs, seqs), 0) == iota((seqs, seqs), 1)
    len_one = jnp.sum(jnp.where(same, lengths[...].astype(F32), 0.0), axis=1, keepdims=True)
    len_col = jnp.concatenate([len_one] * heads, axis=0)
    block_len = 256 if k_cols % 256 == 0 else k_cols
    later = onehot(iota((block_len, block_len), 0) > iota((block_len, block_len), 1))
    position = iota((rows, block_len), 1).astype(F32)
    weights = []
    offset = jnp.zeros((rows, 1), F32)
    for a in range(k_parts):
        for c in k_loads[a]:
            c.wait()
        first_col = (k_parts - 1 - a) * k_cols
        scores = dot(diag, kbuf[:, :, first_col:first_col + k_cols].reshape(depth, k_cols)) + bias_col
        for j in reversed(range(k_cols // block_len)):
            s = scores[:, j * block_len:(j + 1) * block_len]
            inside = position < len_col - float(first_col + j * block_len)
            soft = jnp.log(1.0 + jnp.exp(-jnp.abs(s)))
            fall = jnp.where(inside, -(jnp.maximum(s, 0.0) + soft), 0.0)
            rise = jnp.minimum(s, 0.0) - soft
            high = fall.astype(BF16)
            low = (fall - high.astype(F32)).astype(BF16)
            both = dot(jnp.concatenate([high, low], axis=0), later)
            after = both[:rows] + both[rows:]
            w = jnp.exp(rise + (after + offset))
            weights.insert(0, jnp.where(inside, w, 0.0).astype(BF16))
            offset = offset + after[:, 0:1] + fall[:, 0:1]
    weights = jnp.concatenate(weights, axis=1)

    loads["wo"].start()
    for name in ("wk", "wv", "fgain", "routes", "weights", "wg", "wu", "wd"):
        loads[name].start()
    folded = [jnp.zeros((seqs, lanes), F32) for _ in range(heads)]
    per_group = max(1, 256 // head)
    for c in v_loads:
        c.wait()
    for g in range(seqs // per_group):
        found = dot_nt(weights, vbuf[g * per_group:(g + 1) * per_group].reshape(per_group * head, span))
        for c in range(per_group // per):
            m = masks[g * (per_group // per) + c]
            for h in range(heads):
                folded[h] = folded[h] + jnp.where(
                    m, found[h * seqs:(h + 1) * seqs, c * lanes:(c + 1) * lanes], 0.0)
    attended = []
    for p in range(heads // per):
        mine = jnp.zeros((seqs, lanes), F32)
        for j in range(per):
            one = folded[p * per + j]
            full = one
            for t in range(1, per):
                full = full + pltpu.roll(one, t * head, 1)
            mine = jnp.where(block_of == j, full, mine)
        attended.append(mine)
    attended = jnp.concatenate(attended, axis=1).astype(BF16)
    loads["wo"].wait()
    made = dot(attended, wo[...]).astype(BF16)
    part[0] = made[:, :half]
    part[1] = made[:, half:]

    pl.semaphore_wait(barrier, n_tp - 1 + n_ep - 1)
    sends = []
    tp_order = list(range(2, n_tp)) + [1] if n_tp > 2 else [1]

    def tp_peer(d):
        chip = lax.rem(tp // 2 + d // 2, n_tp // 2)
        return 2 * chip + lax.rem(core + d, 2)

    def tp_source(d):
        chip = lax.rem(tp // 2 + n_tp // 2 - d // 2, n_tp // 2)
        return 2 * chip + lax.rem(core + d, 2)

    for d in tp_order:
        peer = tp_peer(d)
        c = pltpu.make_async_remote_copy(
            part.at[lax.rem(core + d, 2)], parts.at[d], a_send.at[d], a_recv.at[d],
            device_id=(ep, peer), device_id_type=MESH)
        c.start()
        sends.append(c)

    loads["routes"].wait()
    loads["weights"].wait()
    loads["wk"].wait()
    loads["wv"].wait()
    slot_rows = iota((total, seqs), 0)
    if pow2:
        expert = jnp.bitwise_xor(slot_rows // cap_pad, ep)
    else:
        expert = lax.rem(slot_rows // cap_pad + ep, n_ep)
    first = routes[0:1, :] == expert
    named = first | (routes[1:2, :] == expert)
    earlier = onehot(iota((seqs, seqs), 0) < iota((seqs, seqs), 1))
    before = dot(onehot(named), earlier)
    planned = jnp.where(named & (before == (slot_rows % cap_pad).astype(F32)), 1.0, 0.0)
    plan = planned.astype(BF16)
    mixing = (planned * jnp.where(first, route_weight[0:1, :], route_weight[1:2, :])).T
    mix_high = mixing.astype(BF16)
    mix_low = (mixing - mix_high.astype(F32)).astype(BF16)
    mix = jnp.concatenate([mix_high.astype(F32), mix_low.astype(F32)], axis=0).astype(BF16)
    new_keys[...] = dot_nt(normed, wk[...]).astype(BF16)
    new_values[...] = dot_nt(normed, wv[...]).astype(BF16)
    at_own = pl.ds(pl.multiple_of(core * half, half), half)
    at_mate = pl.ds(pl.multiple_of((1 - core) * half, half), half)
    attn_total = tokens[:, at_own].astype(F32) + part[core].astype(F32)

    for d in tp_order[::-1]:
        pltpu.make_async_remote_copy(
            part.at[core], parts.at[d], a_send.at[d], a_recv.at[d],
            device_id=(ep, tp_source(d)), device_id_type=MESH).wait_recv()
        attn_total = attn_total + parts[d].astype(F32)
    residual = attn_total.astype(BF16)
    outgoing[...] = dot(plan, residual).astype(BF16).reshape(n_ep, cap_pad, half)

    def cut(ref, k):
        return ref.at[k]

    for k in reversed(range(1, n_ep)):
        c = pltpu.make_async_remote_copy(
            cut(outgoing, k), cut(arrived, k), b_send.at[k], b_recv.at[k],
            device_id=(dest(k), tp), device_id_type=MESH)
        c.start()
        sends.append(c)
    c = pltpu.make_async_remote_copy(
        cut(outgoing, 0), cut(passed, 0), f_send.at[0], f_recv.at[0], device_id=(ep, mate), device_id_type=MESH)
    c.start()
    sends.append(c)
    swaps = [c]
    arrived[0] = outgoing[0]
    loads["fgain"].wait()
    loads["wg"].wait()
    loads["wu"].wait()
    loads["wd"].wait()
    for k in range(1, n_ep):
        pltpu.make_async_remote_copy(
            cut(outgoing, k), cut(arrived, k), b_send.at[k], b_recv.at[k],
            device_id=(source(k), tp), device_id_type=MESH).wait_recv()
        c = pltpu.make_async_remote_copy(
            cut(arrived, k), cut(passed, k), f_send.at[k], f_recv.at[k],
            device_id=(ep, mate), device_id_type=MESH)
        c.start()
        sends.append(c)
        swaps.append(c)
    x = arrived[...].reshape(total, half).astype(F32)
    square = jnp.sum(x * x, axis=-1, keepdims=True)
    x = (x * ffn_gain[:, at_own]).astype(BF16)
    gated = dot(x, wg[at_own, :])
    lifted = dot(x, wu[at_own, :])
    for c in swaps:
        c.wait_recv()
    x = passed[...].reshape(total, half).astype(F32)
    square = square + jnp.sum(x * x, axis=-1, keepdims=True)
    x = (x * ffn_gain[:, at_mate]).astype(BF16)
    factor = lax.rsqrt(square * (1.0 / width) + EPS)
    gated = (gated + dot(x, wg[at_mate, :])) * factor
    lifted = (lifted + dot(x, wu[at_mate, :])) * factor
    hidden = (gated / (1.0 + jnp.exp(-gated)) * lifted).astype(BF16)
    share_out[...] = dot(hidden, wd[:, at_mate]).astype(BF16).reshape(n_ep, cap_pad, half)
    far = n_ep // 2
    pieces = [pl.ds(far, n_ep - far), pl.ds(0, far)]
    pair = []
    for i, piece in enumerate(pieces):
        c = pltpu.make_async_remote_copy(
            share_out.at[piece], share_in.at[piece], c_send.at[i], c_recv.at[i],
            device_id=(ep, mate), device_id_type=MESH)
        c.start()
        sends.append(c)
        pair.append(c)
    own = dot(hidden, wd[:, at_own]).reshape(n_ep, cap_pad, half)
    for i, (lo, hi) in enumerate(((far, n_ep), (0, far))):
        pair[i].wait_recv()
        ret[lo:hi] = (own[lo:hi] + share_in[lo:hi].astype(F32)).astype(BF16)
        for k in reversed(range(max(lo, 1), hi)):
            c = pltpu.make_async_remote_copy(
                cut(ret, k), cut(back, k), d_send.at[k], d_recv.at[k],
                device_id=(source(k), tp), device_id_type=MESH)
            c.start()
            sends.append(c)
    back[0] = ret[0]
    for k in range(1, n_ep):
        pltpu.make_async_remote_copy(
            cut(ret, k), cut(back, k), d_send.at[k], d_recv.at[k],
            device_id=(dest(k), tp), device_id_type=MESH).wait_recv()
    flat = back[...].reshape(total, half)
    both = dot(mix, flat)
    chips = n_tp // 2
    share = (residual.astype(F32) * (1.0 / chips) + (both[:seqs] + both[seqs:])).astype(BF16)
    fin_out[...] = share
    finals[tp] = share
    for d in tp_order:
        c = pltpu.make_async_remote_copy(
            fin_out, finals.at[tp], e_send.at[d], e_recv.at[d],
            device_id=(ep, tp_peer(d)), device_id_type=MESH)
        c.start()
        sends.append(c)
    for d in tp_order[::-1]:
        src = tp_source(d)
        pltpu.make_async_remote_copy(
            fin_out, finals.at[src], e_send.at[d], e_recv.at[d],
            device_id=(ep, src), device_id_type=MESH).wait_recv()
    for c in range(2):
        value = finals[c].astype(F32)
        for x in range(1, chips):
            value = value + finals[2 * x + c].astype(F32)
        mixed[:, c * half:(c + 1) * half] = value.astype(BF16)
    for c in sends:
        c.wait_send()


def finish(mixed_in, keys_in, values_in, mixed, keys, values, sem):
    copies = [
        pltpu.make_async_copy(a, b, sem.at[i])
        for i, (a, b) in enumerate(((mixed_in, mixed), (keys_in, keys), (values_in, values)))
    ]
    for c in copies:
        c.start()
    for c in copies:
        c.wait()


def solution(mesh):
    n_ep, n_tp = mesh.shape["ep"], mesh.shape["tp"]

    def body(tokens, attn_gain, w_query, w_key, w_value, attn_bias, key_cache, value_cache, lengths,
             w_out, ffn_gain, routes, route_weight, gate, up, down):
        seqs, width = tokens.shape
        top = routes.shape[1]
        capacity = max(2, 2 * seqs * top // n_ep)
        cap_pad = -(-capacity // 16) * 16
        half = width // 2
        head = w_key.shape[1]
        units = gate.shape[2]
        vmem = pl.BlockSpec(memory_space=pltpu.VMEM)
        hbm = pl.BlockSpec(memory_space=pl.ANY)
        sem = pltpu.SemaphoreType.DMA
        args = (tokens, attn_gain[None, :], w_query, w_key.T, w_value.T, attn_bias[None, :], key_cache, value_cache,
                lengths[None, :], w_out, ffn_gain[None, :], routes.T, route_weight.T, gate, up, down)
        exchange = pltpu.VMEM((n_ep, cap_pad, half), BF16)
        outs = pl.pallas_call(
            functools.partial(kernel, n_ep, n_tp, capacity, cap_pad),
            out_shape=(
                pltpu.VMEM((seqs, width), BF16),
                pltpu.VMEM((seqs, head), BF16),
                pltpu.VMEM((seqs, head), BF16),
            ),
            in_specs=[hbm] * len(args),
            out_specs=(vmem, vmem, vmem),
            scratch_shapes=[
                pltpu.VMEM(tokens.shape, BF16),
                pltpu.VMEM((1, width), F32),
                pltpu.VMEM((1, attn_bias.shape[0]), F32),
                pltpu.VMEM((1, seqs), jnp.int32),
                pltpu.VMEM((1, width), F32),
                pltpu.VMEM((top, seqs), jnp.int32),
                pltpu.VMEM((top, seqs), F32),
                pltpu.VMEM(w_query.shape, BF16),
                pltpu.VMEM((head, width), BF16),
                pltpu.VMEM((head, width), BF16),
                pltpu.VMEM(key_cache.shape, BF16),
                pltpu.VMEM(value_cache.shape, BF16),
                pltpu.VMEM(w_out.shape, BF16),
                pltpu.VMEM((width, units), BF16),
                pltpu.VMEM((width, units), BF16),
                pltpu.VMEM((units, width), BF16),
                pltpu.VMEM((2, seqs, half), BF16),
                pltpu.VMEM((n_tp, seqs, half), BF16),
                exchange, exchange, exchange, exchange, exchange, exchange, exchange,
                pltpu.VMEM((seqs, half), BF16),
                pltpu.VMEM((n_tp, seqs, half), BF16),
                sem((14,)), sem((2, 3)), sem((3,)),
                sem((n_tp,)), sem((n_tp,)), sem((n_ep,)), sem((n_ep,)), sem((n_ep,)), sem((n_ep,)),
                sem((2,)), sem((2,)), sem((n_ep,)), sem((n_ep,)), sem((n_tp,)), sem((n_tp,)),
            ],
            compiler_params=pltpu.CompilerParams(
                collective_id=0, has_side_effects=True, vmem_limit_bytes=60 * 1024 * 1024),
        )(*args)
        return pl.pallas_call(
            finish,
            out_shape=tuple(jax.ShapeDtypeStruct(x.shape, x.dtype) for x in outs),
            in_specs=[vmem] * 3,
            out_specs=(hbm,) * 3,
            scratch_shapes=[sem((3,))],
        )(*[pltpu.with_memory_space_constraint(x, pltpu.VMEM) for x in outs])

    return jax.shard_map(
        body,
        mesh=mesh,
        in_specs=(
            P("ep", None), P(), P(None, "tp"), P(None, "tp"), P(None, "tp"), P("tp"),
            P("ep", "tp", None), P("ep", "tp", None), P("ep"), P("tp", None), P(),
            P("ep", None), P("ep", None),
            P("ep", None, "tp"), P("ep", None, "tp"), P("ep", "tp", None),
        ),
        out_specs=(P("ep", None), P("ep", "tp"), P("ep", "tp")),
        check_vma=False,
    )
```

time: 37.8 us -> 28.9 us (0.76)
  Pallas kernels: 37 us -> 28.2 us
    pallas_call x1, Pallas kernels: 35.5 us -> 27.5 us  [body(): pl.pallas_call(functools.partial(kernel, n_ep, n_tp, capacity, cap_pad),...]
    pallas_call x1, Pallas kernels: 1.45 us -> 0.65 us  [body(): pl.pallas_call(finish, out_shape=tuple((jax.ShapeDtypeStruct(x.shape, x.d...]
where the time goes in v1:
time: 28.9 us; the launch traced here: 28.8 us
  Pallas kernels  28.2 us (98%)
  between operations  0.65 us (2%)
    pallas_call x1, Pallas kernels, body(): pl.pallas_call(functools.partial(kernel, n_ep, n_tp, capacity, cap_pad),...  27.5 us
    pallas_call x1, Pallas kernels, body(): pl.pallas_call(finish, out_shape=tuple((jax.ShapeDtypeStruct(x.shape, x.d...  0.65 us

profile of v1, /device:TPU:0, one launch (start us, length us, event | category | flops | bytes accessed | tf_op | source)
XLA Modules:
  0.0 28.8 jit_solution(7904241675188860578)
XLA Ops:
  0.6 27.5 %shard_map.175 = (bf16[24,1024]{1,0:T(8,128)(2,1)S(1)}, bf16[24,64]{1,0:T(8,128)(2,1)S(1)}, bf16[24,64]{1,0:T(8,128)(2,1)S(1)}) custom-call(bf16[24,1024]{1,0:T(8,128)(2,1)} %tokens_hbm.1, f32[1,1024]{1,0:T(1,128)} %bitcast.10, bf16[1024,256]{1,0:T(8,128)(2,1)} %w_query.1, bf16[64,1024]{1,0:T(8,128)(2,1)} %bitcast.8, bf16[64,1024]{1,0:T(8,128)(2,1)} %bitcast.9, ...), custom_call_target="tpu_custom_call" | custom-call | tf_op jit(solution)/shard_map/pallas_call | solution.py:377
  28.1 0.7 %shard_map.176 = (bf16[24,1024]{1,0:T(8,128)(2,1)}, bf16[24,64]{1,0:T(8,128)(2,1)}, bf16[24,64]{1,0:T(8,128)(2,1)}) custom-call(bf16[24,1024]{1,0:T(8,128)(2,1)S(1)} %get-tuple-element.6.mixed_in, bf16[24,64]{1,0:T(8,128)(2,1)S(1)} %get-tuple-element.7.keys_in, bf16[24,64]{1,0:T(8,128)(2,1)S(1)} %get-tuple-element.8.values_in), custom_call_target="tpu_custom_call" | custom-call | tf_op jit(solution)/shard_map/pallas_call | solution.py:415
